TPU v7x, 128 devices: a whole 4x4x4 slice. The times are simulated.
128 devices in a mesh: sp: 16 (over z, y), dp: 8 (over x, core).
Axes of the slice: x: 4, y: 4, z: 4, core: 2. Of those that a mesh axis runs over, the one named last changes fastest.
Arguments:
- queries: bfloat16 [8, 2048, 16, 128], P('dp', 'sp'), may hold values from -7 to 7
- key_vectors: bfloat16 [8, 2048, 16, 128], P('dp', 'sp'), may hold values from -6 to 6
- value_vectors: bfloat16 [8, 2048, 16, 128], P('dp', 'sp'), may hold values from -6 to 6
- head_lambda: float32 [16], P('sp'), may hold values from 0.3 to 0.8
- head_gain: float32 [128], replicated, may hold values from 0.1 to 1.9
- residual: bfloat16 [8, 2048, 2048], P('dp', 'sp'), may hold values from -6 to 6
- out_weight: bfloat16 [2048, 2048], replicated, may hold values from -0.125 to 0.125
- mix_gain: float32 [2048], replicated, may hold values from 0.1 to 1.9
- pre_gain: float32 [2048], replicated, may hold values from 0.1 to 1.9
- post_gain: float32 [2048], replicated, may hold values from 0.1 to 1.9
- routes: int32 [8, 2048, 4], P('dp', 'sp'), may hold values from 0 to 127, all different within a row; in each aligned block of 128 rows (0 to 127, 128 to 255, ..., all dimensions but the last counted through in order) at most 6 rows name the same one
- route_weights: float32 [8, 2048, 4], P('dp', 'sp'), may hold values from 0.25 to 1
- expert_gate: bfloat16 [128, 2048, 512], P(('sp', 'dp')), may hold values from -0.125 to 0.125
- expert_up: bfloat16 [128, 2048, 512], P(('sp', 'dp')), may hold values from -0.125 to 0.125
- expert_down: bfloat16 [128, 512, 2048], P(('sp', 'dp')), may hold values from -0.25 to 0.25
- shared_gate: bfloat16 [2048, 512], replicated, may hold values from -0.125 to 0.125
- shared_up: bfloat16 [2048, 512], replicated, may hold values from -0.125 to 0.125
- shared_down: bfloat16 [512, 2048], replicated, may hold values from -0.25 to 0.25
Outputs:
- output: bfloat16 [8, 2048, 2048], P('dp', 'sp')
Inputs may be any that keep to these rules, and one draw needn't show every extreme that they name: `routes`: among the tokens of one device (aligned blocks of 128 positions), no expert is named more than 6 times; in some block some expert is named exactly 6 times. Each token names 4 different experts.
All inputs are finite; a program needn't handle non-finite values.
Results may differ from a plain program's by a relative error of at most 0.0075.
Values may be sent and summed in bfloat16 or wider, within the bound.
A program may use at most 128 MiB of HBM per device.

v0:
```python
import jax
import jax.numpy as jnp
from jax import lax
from jax.sharding import PartitionSpec as P

epsilon = 1e-06


def in_one_piece(arrays, axis, split_dim, concat_dim, along):
    ends, at = ([], 0)
    for a in arrays[:-1]:
        at += a.shape[along]
        ends.append(at)
    both = jnp.concatenate(arrays, axis=along)
    return tuple(
        jnp.split(
            lax.all_to_all(both, axis, split_axis=split_dim, concat_axis=concat_dim, tiled=True),
            ends,
            axis=along,
        )
    )


def rms_scale(values_in, gain):
    return (
        values_in
        * lax.rsqrt(jnp.mean(values_in * values_in, axis=-1, keepdims=True) + epsilon)
        * gain
    )


def feed_forward(rows, gate_w, up_w, down_w):
    gate_val = jnp.dot(rows, gate_w, preferred_element_type=jnp.float32)
    up_val = jnp.dot(rows, up_w, preferred_element_type=jnp.float32)
    hidden = (jax.nn.silu(gate_val) * up_val).astype(jnp.bfloat16)
    return jnp.dot(hidden, down_w, preferred_element_type=jnp.float32).astype(jnp.bfloat16)


def attend_heads(query_heads, key_heads, value_heads, head_lambda, head_gain):
    length = query_heads.shape[0]
    head_count = query_heads.shape[1]
    head_size = query_heads.shape[2] // 2
    block_rows = min(512, length)
    block_count = length // block_rows
    query_blocks = query_heads.reshape(block_count, block_rows, head_count, 2, head_size)
    key_all = key_heads.reshape(length, head_count, 2, head_size)
    key_pos = jnp.arange(length, dtype=jnp.int32)

    def one_block(inputs):
        query_block, block_index = inputs
        scores = jnp.einsum(
            "qhmd,khmd->hmqk", query_block, key_all, preferred_element_type=jnp.float32
        ) * head_size ** (-0.5)
        query_pos = block_index * block_rows + jnp.arange(block_rows, dtype=jnp.int32)
        causal = key_pos[None, :] <= query_pos[:, None]
        scores = jnp.where(causal, scores, -jnp.inf)
        maxima = jnp.max(scores, axis=-1, keepdims=True)
        exponent = jnp.exp(scores - maxima)
        softmax_both = exponent / jnp.sum(exponent, axis=-1, keepdims=True)
        mixture = (softmax_both[:, 0] - head_lambda[:, None, None] * softmax_both[:, 1]).astype(
            jnp.bfloat16
        )
        head_output = jnp.einsum(
            "hqk,khe->qhe", mixture, value_heads, preferred_element_type=jnp.float32
        )
        return rms_scale(head_output, head_gain).astype(jnp.bfloat16)

    outputs = lax.map(one_block, (query_blocks, jnp.arange(block_count, dtype=jnp.int32)))
    return outputs.reshape(length, head_count, -1)


def local(
    queries,
    key_vectors,
    value_vectors,
    head_lambda,
    head_gain,
    residual,
    out_weight,
    mix_gain,
    pre_gain,
    post_gain,
    routes,
    route_weights,
    expert_gate,
    expert_up,
    expert_down,
    shared_gate,
    shared_up,
    shared_down,
):
    query_heads, key_heads, value_heads = in_one_piece(
        (queries[0], key_vectors[0], value_vectors[0]), "sp", 1, 0, 2
    )
    attended = attend_heads(query_heads, key_heads, value_heads, head_lambda, head_gain)
    token_heads = lax.all_to_all(attended, "sp", split_axis=0, concat_axis=1, tiled=True)
    tok_count = token_heads.shape[0]
    flat_heads = token_heads.reshape(tok_count, -1)
    mixed_rows = jnp.dot(flat_heads, out_weight, preferred_element_type=jnp.float32)
    updated = (residual[0].astype(jnp.float32) + rms_scale(mixed_rows, mix_gain)).astype(
        jnp.bfloat16
    )
    normed = rms_scale(updated.astype(jnp.float32), pre_gain).astype(jnp.bfloat16)
    model_width = normed.shape[1]
    experts_total = lax.axis_size("sp") * lax.axis_size("dp")
    top_count = routes.shape[2]
    capacity = 3 * tok_count * top_count // (2 * experts_total)
    assign_count = tok_count * top_count
    flat_routes = routes[0].reshape(assign_count)
    one_hot = (flat_routes[:, None] == jnp.arange(experts_total, dtype=jnp.int32)[None, :]).astype(
        jnp.int32
    )
    earlier = jnp.cumsum(one_hot, axis=0) - one_hot
    rank_index = jnp.sum(earlier * one_hot, axis=1)
    slot_index = flat_routes * capacity + rank_index
    source_row = (
        jnp.zeros((experts_total * capacity,), jnp.int32)
        .at[slot_index]
        .set(jnp.arange(assign_count, dtype=jnp.int32) // top_count)
    )
    occupied = (
        jnp.zeros((experts_total * capacity,), jnp.bfloat16)
        .at[slot_index]
        .set(jnp.ones((assign_count,), jnp.bfloat16))
    )
    outgoing = (normed[source_row] * occupied[:, None]).reshape(
        experts_total, capacity, model_width
    )
    shared_out = feed_forward(normed, shared_gate, shared_up, shared_down)
    arrived = lax.all_to_all(outgoing, ("sp", "dp"), split_axis=0, concat_axis=0, tiled=True)
    flat_rows = arrived.reshape(-1, model_width)
    result_rows = feed_forward(flat_rows, expert_gate[0], expert_up[0], expert_down[0])
    results = result_rows.reshape(arrived.shape[0], -1, model_width)
    returned = lax.all_to_all(results, ("sp", "dp"), split_axis=0, concat_axis=0, tiled=True)
    picked = returned.reshape(experts_total * capacity, model_width)[slot_index]
    routed = jnp.sum(
        picked.astype(jnp.float32).reshape(tok_count, top_count, model_width)
        * route_weights[0][:, :, None],
        axis=1,
    )
    combined = routed + shared_out.astype(jnp.float32)
    output = (updated.astype(jnp.float32) + rms_scale(combined, post_gain)).astype(jnp.bfloat16)
    return output.reshape(1, tok_count, model_width)


def solution(mesh):
    in_specs = (
        P("dp", "sp", None, None),
        P("dp", "sp", None, None),
        P("dp", "sp", None, None),
        P("sp"),
        P(),
        P("dp", "sp", None),
        P(),
        P(),
        P(),
        P(),
        P("dp", "sp", None),
        P("dp", "sp", None),
        P(("sp", "dp"), None, None),
        P(("sp", "dp"), None, None),
        P(("sp", "dp"), None, None),
        P(),
        P(),
        P(),
    )
    out_specs = P("dp", "sp", None)
    return jax.shard_map(local, mesh=mesh, in_specs=in_specs, out_specs=out_specs, check_vma=False)
```

profile of v0, /device:TPU:1, one launch (start us, length us, event | category | flops | bytes accessed | tf_op | source)
XLA Modules:
  0.0 325.8 jit_solution(11431756726832329414)
XLA Ops:
  4.2 8.6 %all-to-all-start = ((bf16[128,16,384]{2,0,1:T(8,128)(2,1)}), bf16[128,16,384]{2,0,1:T(8,128)(2,1)}, u32[]{:S(2)}, u32[]{:S(2)}) async-start(bf16[128,16,384]{2,0,1:T(8,128)(2,1)} %pad_maximum_fusion), calls=%async_computation | async-start | bytes 3145728 | tf_op jit(solution)/shard_map/all_to_all | solution.py:17
  14.1 21.9 %all-to-all-done = bf16[128,16,384]{2,0,1:T(8,128)(2,1)} async-done(((bf16[128,16,384]{2,0,1:T(8,128)(2,1)}), bf16[128,16,384]{2,0,1:T(8,128)(2,1)}, u32[]{:S(2)}, u32[]{:S(2)}) %all-to-all-start) | async-done | bytes 1572896 | tf_op jit(solution)/shard_map/all_to_all | solution.py:17
  44.9 62.9 %while.11 = (s32[]{:T(128)}, bf16[4,512,1,128]{3,1,0,2:T(8,128)(2,1)}, s32[4]{0:T(128)S(1)}, bf16[4,512,1,2,64]{1,4,3,2,0:T(8,128)(2,1)}, bf16[2048,1,2,64]{0,3,...) while((s32[]{:T(128)}, ...), condition=%wide.region_4.5_spmd.clone, body=%wide.region_0.4_spmd.clone.sunk | while | flops 549788672 | bytes 21247620 | solution.py:68
  46.9 7.8 %divide_bitcast_fusion.2 = f32[1,2,512,2048]{3,2,1,0:T(8,128)} fusion(pred[512,2048]{1,0:T(8,128)(4,1)S(1)} %iota_compare_fusion.5, bf16[2048,1,2,64]{0,3,2,1:T(8,128)(2,1)} %get-tuple-element.193, bf16[4,512,1,2,64]{1,4,3,2,0:T(8,128)(2,1)} %get-tuple-element.192, s32[]{:T(128)} %get-tuple-element.179), kind=kOutput, calls=%fused_computation.7.clone.1 | convolution fusion | flops 276830208 | bytes 10093056 | tf_op jit(solution)/shard_map/while/body/eval_jaxpr/div | solution.py:59
  54.7 5.0 %multiply_reduce_fusion.5 = (f32[512]{0:T(512)S(1)}, f32[1,128,512]{2,1,0:T(8,128)S(1)}) fusion(bf16[2048,1,128]{2,0,1:T(8,128)(2,1)} %get-tuple-element.195, f32[1,2,512,2048]{3,2,1,0:T(8,128)} %divide_bitcast_fusion.2, f32[]{:T(128)} %bitcast.127), kind=kOutput, calls=%fused_computation.27.clone.1 | convolution fusion | flops 271711744 | bytes 9177092 | tf_op jit(solution)/shard_map/while/body/eval_jaxpr/hqk,khe->qhe/dot_general | solution.py:63
  62.7 7.8 %divide_bitcast_fusion.2 = f32[1,2,512,2048]{3,2,1,0:T(8,128)} fusion(pred[512,2048]{1,0:T(8,128)(4,1)S(1)} %iota_compare_fusion.5, bf16[2048,1,2,64]{0,3,2,1:T(8,128)(2,1)} %get-tuple-element.193, bf16[4,512,1,2,64]{1,4,3,2,0:T(8,128)(2,1)} %get-tuple-element.192, s32[]{:T(128)} %get-tuple-element.179), kind=kOutput, calls=%fused_computation.7.clone.1 | convolution fusion | flops 276830208 | bytes 10093056 | tf_op jit(solution)/shard_map/while/body/eval_jaxpr/div | solution.py:59
  70.5 5.0 %multiply_reduce_fusion.5 = (f32[512]{0:T(512)S(1)}, f32[1,128,512]{2,1,0:T(8,128)S(1)}) fusion(bf16[2048,1,128]{2,0,1:T(8,128)(2,1)} %get-tuple-element.195, f32[1,2,512,2048]{3,2,1,0:T(8,128)} %divide_bitcast_fusion.2, f32[]{:T(128)} %bitcast.127), kind=kOutput, calls=%fused_computation.27.clone.1 | convolution fusion | flops 271711744 | bytes 9177092 | tf_op jit(solution)/shard_map/while/body/eval_jaxpr/hqk,khe->qhe/dot_general | solution.py:63
  78.4 7.8 %divide_bitcast_fusion.2 = f32[1,2,512,2048]{3,2,1,0:T(8,128)} fusion(pred[512,2048]{1,0:T(8,128)(4,1)S(1)} %iota_compare_fusion.5, bf16[2048,1,2,64]{0,3,2,1:T(8,128)(2,1)} %get-tuple-element.193, bf16[4,512,1,2,64]{1,4,3,2,0:T(8,128)(2,1)} %get-tuple-element.192, s32[]{:T(128)} %get-tuple-element.179), kind=kOutput, calls=%fused_computation.7.clone.1 | convolution fusion | flops 276830208 | bytes 10093056 | tf_op jit(solution)/shard_map/while/body/eval_jaxpr/div | solution.py:59
  86.2 5.0 %multiply_reduce_fusion.5 = (f32[512]{0:T(512)S(1)}, f32[1,128,512]{2,1,0:T(8,128)S(1)}) fusion(bf16[2048,1,128]{2,0,1:T(8,128)(2,1)} %get-tuple-element.195, f32[1,2,512,2048]{3,2,1,0:T(8,128)} %divide_bitcast_fusion.2, f32[]{:T(128)} %bitcast.127), kind=kOutput, calls=%fused_computation.27.clone.1 | convolution fusion | flops 271711744 | bytes 9177092 | tf_op jit(solution)/shard_map/while/body/eval_jaxpr/hqk,khe->qhe/dot_general | solution.py:63
  94.1 7.8 %divide_bitcast_fusion.2 = f32[1,2,512,2048]{3,2,1,0:T(8,128)} fusion(pred[512,2048]{1,0:T(8,128)(4,1)S(1)} %iota_compare_fusion.5, bf16[2048,1,2,64]{0,3,2,1:T(8,128)(2,1)} %get-tuple-element.193, bf16[4,512,1,2,64]{1,4,3,2,0:T(8,128)(2,1)} %get-tuple-element.192, s32[]{:T(128)} %get-tuple-element.179), kind=kOutput, calls=%fused_computation.7.clone.1 | convolution fusion | flops 276830208 | bytes 10093056 | tf_op jit(solution)/shard_map/while/body/eval_jaxpr/div | solution.py:59
  101.9 5.0 %multiply_reduce_fusion.5 = (f32[512]{0:T(512)S(1)}, f32[1,128,512]{2,1,0:T(8,128)S(1)}) fusion(bf16[2048,1,128]{2,0,1:T(8,128)(2,1)} %get-tuple-element.195, f32[1,2,512,2048]{3,2,1,0:T(8,128)} %divide_bitcast_fusion.2, f32[]{:T(128)} %bitcast.127), kind=kOutput, calls=%fused_computation.27.clone.1 | convolution fusion | flops 271711744 | bytes 9177092 | tf_op jit(solution)/shard_map/while/body/eval_jaxpr/hqk,khe->qhe/dot_general | solution.py:63
  130.0 4.8 %multiply_reduce_fusion.3 = (f32[128]{0:T(128)S(1)}, f32[128,2048]{1,0:T(8,128)S(1)}) fusion(bf16[128,2048]{0,1:T(8,128)(2,1)S(1)} %bitcast.128, bf16[2048,2048]{1,0:T(8,128)(2,1)} %param.26), kind=kOutput, calls=%fused_computation.65 | convolution fusion | flops 1074265984 | bytes 9961984 | tf_op jit(solution)/shard_map/dot_general | solution.py:99
  139.7 6.3 %gather.9 = bf16[128,6,2048]{2,1,0:T(8,128)(2,1)} reshape(bf16[768,2048]{1,0:T(8,128)(2,1)} %gather_fusion) | data formatting | bytes 6291456 | tf_op jit(solution)/shard_map/gather | solution.py:126
  148.5 61.0 %all_to_all.43 = bf16[128,6,2048]{2,1,0:T(8,128)(2,1)} all-to-all(bf16[128,6,2048]{2,1,0:T(8,128)(2,1)S(1)} %broadcast_multiply_fusion), channel_id=1, replica_groups=mesh['sp'=16,'dp'=8] {'sp','dp'}, dimensions={0} | all-to-all | bytes 6291456 | tf_op jit(solution)/shard_map/all_to_all | solution.py:130
  209.5 6.3 %reshape.181 = bf16[768,2048]{1,0:T(8,128)(2,1)} reshape(bf16[128,6,2048]{2,1,0:T(8,128)(2,1)} %all_to_all.43) | data formatting | bytes 6291456 | tf_op jit(solution)/shard_map/reshape | solution.py:131
  215.8 5.6 %fusion.46 = f32[768,512]{1,0:T(8,128)} fusion(bf16[768,2048]{1,0:T(8,128)(2,1)} %reshape.181, bf16[1,2048,512]{2,1,0:T(8,128)(2,1)} %param.32), kind=kOutput, calls=%fused_computation.48 | convolution fusion | flops 1610612736 | bytes 6815744 | tf_op jit(solution)/shard_map/dot_general | solution.py:33
  221.4 8.1 %convolution_convert_fusion = bf16[768,2048]{1,0:T(8,128)(2,1)} fusion(bf16[1,512,2048]{2,1,0:T(8,128)(2,1)S(1)} %copy-done, f32[768,512]{1,0:T(8,128)} %fusion.46, bf16[768,2048]{1,0:T(8,128)(2,1)} %reshape.181, bf16[1,2048,512]{2,1,0:T(8,128)(2,1)} %param.33), kind=kOutput, calls=%fused_computation.41 | convolution fusion | flops 3225157632 | bytes 12058624 | tf_op jit(solution)/shard_map/dot_general | solution.py:36
  229.5 6.3 %reshape.182 = bf16[128,6,2048]{2,1,0:T(8,128)(2,1)} reshape(bf16[768,2048]{1,0:T(8,128)(2,1)} %convolution_convert_fusion) | data formatting | bytes 6291456 | tf_op jit(solution)/shard_map/reshape | solution.py:133
  235.8 5.7 %all-to-all-start.3 = ((bf16[128,6,2048]{2,1,0:T(8,128)(2,1)}), bf16[128,6,2048]{2,1,0:T(8,128)(2,1)}, u32[]{:S(2)}, u32[]{:S(2)}) async-start(bf16[128,6,2048]{2,1,0:T(8,128)(2,1)} %reshape.182), calls=%async_computation.3 | async-start | bytes 8388608 | tf_op jit(solution)/shard_map/all_to_all | solution.py:134
  243.6 50.5 %all-to-all-done.3 = bf16[128,6,2048]{2,1,0:T(8,128)(2,1)} async-done(((bf16[128,6,2048]{2,1,0:T(8,128)(2,1)}), bf16[128,6,2048]{2,1,0:T(8,128)(2,1)}, u32[]{:S(2)}, u32[]{:S(2)}) %all-to-all-start.3) | async-done | bytes 3145760 | tf_op jit(solution)/shard_map/all_to_all | solution.py:134
  294.2 6.3 %reshape.183 = bf16[768,2048]{1,0:T(8,128)(2,1)} reshape(bf16[128,6,2048]{2,1,0:T(8,128)(2,1)} %all-to-all-done.3) | data formatting | bytes 6291456 | tf_op jit(solution)/shard_map/reshape | solution.py:135
  300.5 7.6 %gather_fusion.1 = bf16[512,2048]{1,0:T(8,128)(2,1)} fusion(bf16[768,2048]{1,0:T(8,128)(2,1)} %reshape.183, s32[1024]{0:T(1024)S(1)} %pad_clamp_fusion), kind=kCustom, calls=%fused_computation.1 | custom fusion | bytes 4196352 | tf_op jit(solution)/shard_map/gather | solution.py:135
  308.1 4.8 %reshape.186 = f32[128,4,2048]{2,1,0:T(4,128)} reshape(bf16[512,2048]{1,0:T(8,128)(2,1)} %gather_fusion.1) | data formatting | bytes 6291456 | tf_op jit(solution)/shard_map/convert_element_type | solution.py:137
  312.9 6.3 %multiply_reduce_fusion.1 = f32[128,2048]{1,0:T(8,128)} fusion(f32[128,4,2048]{2,1,0:T(4,128)} %reshape.186, f32[128,4]{1,0:T(8,128)S(1)} %copy.49), kind=kLoop, calls=%fused_computation.40 | loop fusion | flops 1835008 | bytes 5244928 | tf_op jit(solution)/shard_map/reduce_sum | solution.py:136
  (96 shorter events, 61.4 us)
Async XLA Ops:
  0.0 221.4 %copy-start = (bf16[1,512,2048]{2,1,0:T(8,128)(2,1)S(1)}, bf16[1,512,2048]{2,1,0:T(8,128)(2,1)}, u32[]{:S(2)}) copy-start(bf16[1,512,2048]{2,1,0:T(8,128)(2,1)} %param.34) | copy-start | bytes 6291460
  2.8 10.1 %copy-start.6 = (s32[1,128,4]{1,2,0:T(4,128)S(1)}, s32[1,128,4]{1,2,0:T(4,128)}, u32[]{:S(2)}) copy-start(s32[1,128,4]{1,2,0:T(4,128)} %param.30) | copy-start | bytes 6148
  4.2 31.8 %all-to-all-start = ((bf16[128,16,384]{2,0,1:T(8,128)(2,1)}), bf16[128,16,384]{2,0,1:T(8,128)(2,1)}, u32[]{:S(2)}, u32[]{:S(2)}) async-start(bf16[128,16,384]{2,0,1:T(8,128)(2,1)} %pad_maximum_fusion), calls=%async_computation | async-start | bytes 3145728 | tf_op jit(solution)/shard_map/all_to_all | solution.py:17
  36.0 8.9 %copy-start.2 = (f32[128]{0:T(128)S(1)}, f32[128]{0:T(128)}, u32[]{:S(2)}) copy-start(f32[128]{0:T(128)} %param.24) | copy-start | bytes 1540
  111.4 14.2 %all-to-all-start.1 = ((bf16[16,2,8192]{2,1,0:T(2,128)(2,1)}), bf16[16,2,8192]{2,1,0:T(2,128)(2,1)}, u32[]{:S(2)}, u32[]{:S(2)}) async-start(bf16[16,2,8192]{2,1,0:T(2,128)(2,1)} %reshape.228), calls=%async_computation.1 | async-start | bytes 1048576 | tf_op jit(solution)/shard_map/all_to_all | solution.py:96
  130.0 4.8 %copy-start.1 = (bf16[1,128,2048]{2,1,0:T(8,128)(2,1)S(1)}, bf16[1,128,2048]{2,1,0:T(8,128)(2,1)}, u32[]{:S(2)}) copy-start(bf16[1,128,2048]{2,1,0:T(8,128)(2,1)} %param.25) | copy-start | bytes 1572868
  130.0 4.8 %copy-start.3 = (f32[2048]{0:T(1024)S(1)}, f32[2048]{0:T(1024)}, u32[]{:S(2)}) copy-start(f32[2048]{0:T(1024)} %param.27) | copy-start | bytes 24580
  130.0 5.2 %copy-start.4 = (f32[2048]{0:T(1024)S(1)}, f32[2048]{0:T(1024)}, u32[]{:S(2)}) copy-start(f32[2048]{0:T(1024)} %param.28) | copy-start | bytes 24580
  235.8 5.7 %copy-start.7 = (f32[1,128,4]{1,2,0:T(4,128)S(1)}, f32[1,128,4]{1,2,0:T(4,128)}, u32[]{:S(2)}) copy-start(f32[1,128,4]{1,2,0:T(4,128)} %param.31) | copy-start | bytes 6148
  235.8 58.4 %all-to-all-start.3 = ((bf16[128,6,2048]{2,1,0:T(8,128)(2,1)}), bf16[128,6,2048]{2,1,0:T(8,128)(2,1)}, u32[]{:S(2)}, u32[]{:S(2)}) async-start(bf16[128,6,2048]{2,1,0:T(8,128)(2,1)} %reshape.182), calls=%async_computation.3 | async-start | bytes 8388608 | tf_op jit(solution)/shard_map/all_to_all | solution.py:134
  319.2 4.4 %copy-start.5 = (f32[2048]{0:T(1024)S(1)}, f32[2048]{0:T(1024)}, u32[]{:S(2)}) copy-start(f32[2048]{0:T(1024)} %param.29) | copy-start | bytes 24580
where the time goes:
time: 327 us; the launch traced here: 326 us
  matrix products  76 us (23%)
  waiting for transfers between devices  75.5 us (23%)
  local copies, waits for them, and re-layouts  72.6 us (22%)
  blocking collectives  61 us (19%)
  starting transfers between devices  18.8 us (6%)
  other arithmetic  18.7 us (6%)
    all_to_all x1, blocking collectives, local(): lax.all_to_all(outgoing, ('sp', 'dp'), split_axis=0, concat_axis=0, tiled...  61 us
    all_to_all x1, waiting for transfers between devices, local(): lax.all_to_all(results, ('sp', 'dp'), split_axis=0, concat_axis=0, tiled=...  50.5 us
    div x4, matrix products, one_block(): softmax_both = exponent / jnp.sum(exponent, axis=-1, keepdims=True)  31.2 us
    all_to_all x1, waiting for transfers between devices, in_one_piece(): lax.all_to_all(both, axis, split_axis=split_dim, concat_axis=concat_dim,...  21.9 us
    dot_general x4, matrix products, one_block(): jnp.einsum('hqk,khe->qhe', mixture, value_heads, preferred_element_type=j...  19.9 us
    dot_general x2, matrix products, feed_forward(): jnp.dot(hidden, down_w, preferred_element_type=jnp.float32)  12.5 us
    gather x2, local copies, waits for them, and re-layouts, local(): normed[source_row] * occupied[:, None]  10.5 us
    all_to_all x1, starting transfers between devices, in_one_piece(): lax.all_to_all(both, axis, split_axis=split_dim, concat_axis=concat_dim,...  8.63 us
  transfers between devices with their start and end apart: 3, of which 3 were waited for; matrix products, arithmetic and copies ran while one was open for 3% of the time, Pallas kernels for 0%

commit v1 on v0

v1 whole, which is shorter than its diff:
```python
import functools

import jax
import jax.numpy as jnp
import numpy as np
from jax import lax
from jax.experimental import pallas as pl
from jax.experimental.pallas import tpu as pltpu
from jax.sharding import PartitionSpec as P

MESH = pl.DeviceIdType.MESH
EPS = 1e-06
F32, BF16, I32 = jnp.float32, jnp.bfloat16, jnp.int32


def digits(k):
    return k // 32, (k // 8) % 4, (k // 2) % 4, k % 2


def link_load(k):
    load = np.zeros(6)
    dz, dy, dx, _ = digits(k)
    for i, d in enumerate((dx, dy, dz)):
        if d in (1, 2):
            load[2 * i] += 1
        if d in (2, 3):
            load[2 * i + 1] += 1
    return load


def first_link(k):
    dz, dy, dx, _ = digits(k)
    for i, d in enumerate((dx, dy, dz)):
        if d:
            return i, d
    return 3, 0


def balanced_order(offsets):
    left, total, out, last = list(offsets), np.zeros(6), [], None
    while left:

        def cost(k):
            t = total + link_load(k)
            return t.max() - t.min() + (0.5 if last is not None and first_link(k) == last else 0)

        k = min(left, key=cost)
        left.remove(k)
        out.append(k)
        total = total + link_load(k)
        last = first_link(k)
    return out


SP_ORDER = [k // 8 for k in balanced_order([8 * s for s in range(1, 16)])]
ALL_ORDER = [0] + balanced_order(range(1, 128))


def shifted(sp, dp, k, sign):
    dz, dy, dx, dc = digits(k)
    if sign < 0:
        dz, dy, dx, dc = -dz % 4, -dy % 4, -dx % 4, -dc % 2
    rem = lax.rem
    nsp = rem(sp // 4 + dz, 4) * 4 + rem(rem(sp, 4) + dy, 4)
    ndp = rem(dp // 2 + dx, 4) * 2 + rem(rem(dp, 2) + dc, 2)
    return nsp, ndp


def landed(ref, sem):
    pltpu.make_async_copy(ref, ref, sem).wait()


def dot(a, b):
    return jnp.dot(a, b, preferred_element_type=F32)


def rms(v, gain):
    return v * lax.rsqrt(jnp.mean(v * v, axis=-1, keepdims=True) + EPS) * gain


def layer_kernel(
    q_ref, k_ref, v_ref, lam_ref, hgain_ref, res_ref, mixg_ref, preg_ref, postg_ref,
    routes_ref, rw_ref, order_ref, perm_ref, permt_ref,
    wo_hbm, eg_hbm, eu_hbm, ed_hbm, sg_hbm, su_hbm, sd_hbm,
    out_ref,
    wo, eg, eu, ed, sg, su, sd,
    spread, qkv_send, qkv_recv, vext, head_send, head_recv, acc,
    x4, pick, slab_send, slab_recv, res_send, res_recv, whi, wlo, xs, upd, shared, r0s,
    wsem, qs_sem, qr_sem, hs_sem, hr_sem, ds_sem, dr_sem, rs_sem, rr_sem,
):
    sp, dp = lax.axis_index("sp"), lax.axis_index("dp")
    loads = [
        pltpu.make_async_copy(src, dst, wsem.at[i])
        for i, (src, dst) in enumerate(
            ((wo_hbm, wo), (sg_hbm, sg), (su_hbm, su), (sd_hbm, sd), (eg_hbm, eg), (eu_hbm, eu), (ed_hbm, ed))
        )
    ]
    barrier = pltpu.get_barrier_semaphore()

    @pl.loop(1, 128)
    def _(k):
        peer = lax.rem(sp * 8 + dp + k, 128)
        pl.semaphore_signal(barrier, inc=1, device_id=(peer // 8, lax.rem(peer, 8)), device_id_type=MESH)

    for part, ref in enumerate((q_ref, k_ref, v_ref)):
        spread[part] = ref[...].reshape(2048, 128).astype(F32)
    for h in range(16):
        for part in range(3):
            qkv_send[h, part] = spread[part, pl.ds(h, 128, stride=16), :].astype(BF16)
    pl.semaphore_wait(barrier, 127)
    for i, d in enumerate(SP_ORDER):
        to, _ = shifted(sp, dp, 8 * d, 1)
        pltpu.make_async_remote_copy(
            qkv_send.at[to], qkv_recv.at[sp], qs_sem.at[i], qr_sem.at[i],
            device_id=(to, dp), device_id_type=MESH,
        ).start()
    for load in loads:
        load.start()
    qkv_recv[sp] = qkv_send[sp]

    oz, oy, ox, oc = (order_ref[i : i + 1, :] for i in range(4))
    mz, my, mx, mc = sp // 4, lax.rem(sp, 4), dp // 2, lax.rem(dp, 2)
    expert = ((oz + mz) & 3) * 32 + ((oy + my) & 3) * 8 + ((ox + mx) & 3) * 2 + ((oc + mc) & 1)
    row_i = lax.broadcasted_iota(I32, (128, 128), 0)
    col_i = lax.broadcasted_iota(I32, (128, 128), 1)
    hots = [routes_ref[:, j : j + 1] == expert for j in range(4)]
    members = sum(h.astype(F32) for h in hots).astype(BF16)
    earlier = dot((col_i < row_i).astype(F32).astype(BF16), members)
    place = earlier + 24.0 * col_i.astype(F32)
    eye = col_i == row_i
    rows_j = []
    for j in range(4):
        r0 = jnp.sum(jnp.where(hots[j], place, 0.0), axis=1, keepdims=True)
        r0s[:, j : j + 1] = r0.astype(I32)
        r0_row = jnp.sum(jnp.where(eye, r0, 0.0), axis=0, keepdims=True).astype(I32)
        rows_j.append(jnp.concatenate([r0_row + 6 * q for q in range(4)], axis=1))

    @pl.loop(0, 24)
    def _(c):
        base = pl.multiple_of(c * 128, 128)
        row = lax.broadcasted_iota(I32, (128, 512), 0) + base
        hit = (row == rows_j[0]) | (row == rows_j[1]) | (row == rows_j[2]) | (row == rows_j[3])
        pick[pl.ds(base, 128), :] = jnp.where(hit, 1.0, 0.0).astype(BF16)

    @pl.loop(0, 24)
    def _(c):
        base = pl.multiple_of(c * 128, 128)
        col = lax.broadcasted_iota(I32, (128, 128), 1) + base
        for q in range(4):
            w = jnp.zeros((128, 128), F32)
            for j in range(4):
                w = w + jnp.where(col == r0s[:, j : j + 1] + 6 * q, rw_ref[:, j : j + 1], 0.0)
            hi = w.astype(BF16)
            whi[pl.ds(q * 128, 128), pl.ds(base, 128)] = hi
            wlo[pl.ds(q * 128, 128), pl.ds(base, 128)] = (w - hi.astype(F32)).astype(BF16)

    vext[:, 128:256] = jnp.ones((2048, 128), BF16)
    for i in range(15):
        landed(qkv_recv.at[0], qr_sem.at[i])
    vext[:, 0:128] = qkv_recv[:, 2].reshape(2048, 128)

    lam = lam_ref[0]
    coef = 0.125 * 1.4426950408889634

    def query_block(i):
        n = i + 1
        qb = qkv_recv[i, 0]
        lane = lax.broadcasted_iota(I32, (128, 128), 1)
        zero = jnp.zeros_like(qb)
        q2 = jnp.concatenate([jnp.where(lane < 64, qb, zero), jnp.where(lane >= 64, qb, zero)], axis=0)
        keys = qkv_recv[0:n, 1].reshape(n * 128, 128)
        s = lax.dot_general(q2, keys, (((1,), (1,)), ((), ())), preferred_element_type=F32)
        r2 = lax.broadcasted_iota(I32, (256, 128), 0) & 127
        c2 = lax.broadcasted_iota(I32, (256, 128), 1)
        diag = jnp.where(c2 <= r2, s[:, i * 128 :], -1e30)
        s = diag if i == 0 else jnp.concatenate([s[:, : i * 128], diag], axis=1)
        m = jnp.max(s, axis=1, keepdims=True)
        p = jnp.exp2((s - m) * coef).astype(BF16)
        ol = dot(p, vext[0 : n * 128, :])
        o = ol[:, 0:128] / ol[:, 128:256]
        return rms(o[0:128] - lam * o[128:256], hgain_ref[...]).astype(BF16)

    @pl.loop(0, 8)
    def _(j):
        a = lax.rem(sp + j, 8)
        for b in range(8):

            @pl.when(a == b)
            def _():
                head_send[b] = query_block(b)
                head_send[15 - b] = query_block(15 - b)

        for to in (a, 15 - a):

            @pl.when(to != sp)
            def _():
                pltpu.make_async_remote_copy(
                    head_send.at[to], head_recv.at[sp], hs_sem.at[to], hr_sem.at[sp],
                    device_id=(to, dp), device_id_type=MESH,
                ).start()

    head_recv[sp] = head_send[sp]

    loads[0].wait()
    own = jnp.where(sp < 8, sp, 15 - sp)
    acc[...] = jnp.zeros_like(acc)

    @pl.loop(0, 8)
    def _(j):
        h0 = lax.rem(own - j + 8, 8)
        for h in (h0, h0 + 8):

            @pl.when(h != sp)
            def _():
                landed(head_recv.at[h], hr_sem.at[h])

        x = jnp.concatenate([head_recv[h0], head_recv[h0 + 8]], axis=1)
        for c in range(4):
            cols = pl.ds(c * 512, 512)
            w = jnp.concatenate([wo[h0, :, cols], wo[h0 + 8, :, cols]], axis=0)
            acc[:, cols] += dot(x, w)

    updated = (res_ref[...].astype(F32) + rms(acc[...], mixg_ref[...])).astype(BF16)
    upd[...] = updated
    normed = rms(updated.astype(F32), preg_ref[...]).astype(BF16)
    for q in range(4):
        x4[q * 128 : (q + 1) * 128, :] = normed[:, q * 512 : (q + 1) * 512]

    for g in range(8):
        rows = dot(pick[g * 384 : (g + 1) * 384, :], x4[...]).astype(BF16)
        slab_send[g * 16 : (g + 1) * 16] = rows.reshape(16, 24, 512)
        for at in range(max(1, 16 * g), 16 * g + 16):
            pltpu.make_async_remote_copy(
                slab_send.at[at], slab_recv.at[at], ds_sem.at[0], dr_sem.at[at // 32],
                device_id=shifted(sp, dp, ALL_ORDER[at], 1), device_id_type=MESH,
            ).start()
    slab_recv[0] = slab_send[0]

    def hidden_of(x, wg, wu):
        gate, up = dot(x, wg), dot(x, wu)
        return (gate / (1.0 + jnp.exp(-gate)) * up).astype(BF16)

    for load in loads[1:]:
        load.wait()
    x4q = [x4[q * 128 : (q + 1) * 128, :] for q in range(4)]
    shared_h = hidden_of(jnp.concatenate(x4q, axis=1), sg[...], su[...])
    shared[...] = dot(shared_h, sd[...]).astype(BF16)

    @pl.loop(0, 4)
    def _(g):
        for gs in range(4):

            @pl.when(g == gs)
            def _():
                lo = max(1, 32 * gs)
                landed(slab_recv.at[pl.ds(lo, 32 * gs + 32 - lo)], dr_sem.at[gs])

        for b in range(4):
            block = slab_recv[pl.ds(g * 32 + b * 8, 8)].reshape(192, 512)
            y = dot(perm_ref[...], block).astype(BF16)
            for q in range(4):
                xs[b * 48 : (b + 1) * 48, q * 512 : (q + 1) * 512] = y[q * 48 : (q + 1) * 48]
        h = hidden_of(xs[...], eg[...], eu[...])
        xs[...] = dot(h, ed[...]).astype(BF16)
        for b in range(4):
            y = jnp.concatenate(
                [xs[b * 48 : (b + 1) * 48, q * 512 : (q + 1) * 512] for q in range(4)], axis=0
            )
            back = dot(permt_ref[...], y).astype(BF16)
            res_send[pl.ds(g * 32 + b * 8, 8)] = back.reshape(8, 24, 512)
        for gs in range(4):

            @pl.when(g == gs)
            def _():
                for at in range(max(1, 32 * gs), 32 * gs + 32):
                    pltpu.make_async_remote_copy(
                        res_send.at[at], res_recv.at[at], rs_sem.at[0], rr_sem.at[gs],
                        device_id=shifted(sp, dp, ALL_ORDER[at], -1), device_id_type=MESH,
                    ).start()

    res_recv[0] = res_send[0]

    mix = acc
    for g in range(4):
        lo = max(1, 32 * g)
        landed(res_recv.at[pl.ds(lo, 32 * g + 32 - lo)], rr_sem.at[g])
        rows = res_recv[g * 32 : (g + 1) * 32].reshape(768, 512)
        cols = pl.ds(g * 768, 768)
        for q in range(4):
            part = dot(whi[pl.ds(q * 128, 128), cols], rows) + dot(wlo[pl.ds(q * 128, 128), cols], rows)
            at = pl.ds(q * 512, 512)
            if g == 0:
                mix[:, at] = part
            else:
                mix[:, at] += part
    combined = mix[...] + shared[...].astype(F32)
    out_ref[...] = (upd[...].astype(F32) + rms(combined, postg_ref[...])).astype(BF16)

    for i in range(15):
        landed(qkv_send.at[0], qs_sem.at[i])
    for i in range(16):

        @pl.when(i != sp)
        def _():
            landed(head_send.at[i], hs_sem.at[i])

    landed(slab_send.at[pl.ds(1, 127)], ds_sem.at[0])
    landed(res_send.at[pl.ds(1, 127)], rs_sem.at[0])


def local(
    queries, key_vectors, value_vectors, head_lambda, head_gain, residual, out_weight, mix_gain, pre_gain,
    post_gain, routes, route_weights, expert_gate, expert_up, expert_down, shared_gate, shared_up, shared_down,
):
    order = np.zeros((8, 128), np.int32)
    order[:4] = np.array([digits(k) for k in ALL_ORDER]).T
    perm = np.zeros((192, 192), np.float32)
    for src in range(8):
        for q in range(4):
            for s in range(6):
                perm[q * 48 + src * 6 + s, src * 24 + q * 6 + s] = 1
    vm, hbm = pl.BlockSpec(memory_space=pltpu.VMEM), pl.BlockSpec(memory_space=pl.ANY)
    dma = pltpu.SemaphoreType.DMA
    slabs = pltpu.VMEM((128, 24, 512), BF16)
    out = pl.pallas_call(
        layer_kernel,
        out_shape=jax.ShapeDtypeStruct((128, 2048), BF16),
        in_specs=[vm, vm, vm, pl.BlockSpec(memory_space=pltpu.SMEM)] + [vm] * 10 + [hbm] * 7,
        out_specs=vm,
        scratch_shapes=[
            pltpu.VMEM((16, 128, 2048), BF16),
            pltpu.VMEM((2048, 512), BF16), pltpu.VMEM((2048, 512), BF16), pltpu.VMEM((512, 2048), BF16),
            pltpu.VMEM((2048, 512), BF16), pltpu.VMEM((2048, 512), BF16), pltpu.VMEM((512, 2048), BF16),
            pltpu.VMEM((3, 2048, 128), F32),
            pltpu.VMEM((16, 3, 128, 128), BF16), pltpu.VMEM((16, 3, 128, 128), BF16),
            pltpu.VMEM((2048, 256), BF16),
            pltpu.VMEM((16, 128, 128), BF16), pltpu.VMEM((16, 128, 128), BF16),
            pltpu.VMEM((128, 2048), F32),
            pltpu.VMEM((512, 512), BF16), pltpu.VMEM((3072, 512), BF16),
            slabs, slabs, slabs, slabs,
            pltpu.VMEM((512, 3072), BF16), pltpu.VMEM((512, 3072), BF16),
            pltpu.VMEM((192, 2048), BF16), pltpu.VMEM((128, 2048), BF16), pltpu.VMEM((128, 2048), BF16),
            pltpu.VMEM((128, 4), I32),
            dma((7,)), dma((15,)), dma((15,)), dma((16,)), dma((16,)), dma((1,)), dma((4,)), dma((1,)), dma((4,)),
        ],
        compiler_params=pltpu.CompilerParams(
            collective_id=0, has_side_effects=True, vmem_limit_bytes=67043328
        ),
    )(
        queries[0], key_vectors[0], value_vectors[0], head_lambda, head_gain.reshape(1, 128), residual[0],
        mix_gain.reshape(1, -1), pre_gain.reshape(1, -1), post_gain.reshape(1, -1), routes[0], route_weights[0],
        jnp.asarray(order), jnp.asarray(perm, BF16), jnp.asarray(perm.T, BF16),
        out_weight.reshape(16, 128, 2048), expert_gate[0], expert_up[0], expert_down[0],
        shared_gate, shared_up, shared_down,
    )
    return out.reshape(1, 128, 2048)


def solution(mesh):
    tokens, heads, experts = P("dp", "sp", None), P("dp", "sp", None, None), P(("sp", "dp"), None, None)
    return jax.shard_map(
        local,
        mesh=mesh,
        in_specs=(
            heads, heads, heads, P("sp"), P(), tokens, P(), P(), P(), P(), tokens, tokens,
            experts, experts, experts, P(), P(), P(),
        ),
        out_specs=tokens,
        check_vma=False,
    )
```

time: 327 us -> 135 us (0.41)
  Pallas kernels: 0 us -> 129 us
  matrix products: 76 us -> 0 us
  waiting for transfers between devices: 75.5 us -> 0 us
  local copies, waits for them, and re-layouts: 72.6 us -> 4.7 us
  blocking collectives: 61 us -> 0 us
  starting transfers between devices: 18.8 us -> 0 us
  other arithmetic: 18.7 us -> 0 us
    pallas_call x0 -> x1, Pallas kernels: none -> 129 us  [local(): pl.pallas_call(layer_kernel, out_shape=jax.ShapeDtypeStruct((128, 2048),...]
    all_to_all x3 -> x0, waiting for transfers between devices: 75.5 us -> none  [the longest x1 50.5 us: local(): lax.all_to_all(results, ('sp', 'dp'), split_axis=0, concat_axis=0, tiled=...]
    all_to_all x1 -> x0, blocking collectives: 61 us -> none  [local(): lax.all_to_all(outgoing, ('sp', 'dp'), split_axis=0, concat_axis=0, tiled...]
    dot_general x9 -> x0, matrix products: 44.8 us -> none  [the longest x4 19.9 us: one_block(): jnp.einsum('hqk,khe->qhe', mixture, value_heads, preferred_element_type=j...]
    div x4 -> x0, matrix products: 31.2 us -> none  [one_block(): softmax_both = exponent / jnp.sum(exponent, axis=-1, keepdims=True)]
    reshape x5 -> x0, local copies, waits for them, and re-layouts: 22 us -> none  [the longest x1 6.33 us: local(): flat_rows = arrived.reshape(-1, model_width)]
    all_to_all x3 -> x0, starting transfers between devices: 18.8 us -> none  [the longest x1 8.63 us: in_one_piece(): lax.all_to_all(both, axis, split_axis=split_dim, concat_axis=concat_dim,...]
    gather x3 -> x0, local copies, waits for them, and re-layouts: 18.1 us -> none  [the longest x2 10.5 us: local(): normed[source_row] * occupied[:, None]]
  transfers between devices with their start and end apart: 3 -> 0, of which waited for: 3 -> 0; matrix products, arithmetic and copies ran while one was open for 3% -> 0% of each run, Pallas kernels for 0% -> 0%
where the time goes in v1:
time: 135 us
  Pallas kernels  129 us (96%)
  local copies, waits for them, and re-layouts  4.7 us (3%)
    pallas_call x1, Pallas kernels, local(): pl.pallas_call(layer_kernel, out_shape=jax.ShapeDtypeStruct((128, 2048),...  129 us
    unnamed x3, local copies, waits for them, and re-layouts  4.7 us

profile of v1, /device:TPU:1, one launch (start us, length us, event | category | flops | bytes accessed | tf_op | source)
XLA Modules:
  0.0 134.8 jit_solution(2722654248729525282)
XLA Ops:
  0.7 1.4 %copy.22 = s32[1,128,4]{2,1,0:T(8,128)} copy(s32[1,128,4]{1,2,0:T(4,128)} %param.31) | data formatting | bytes 4096 | tf_op args[10]
  2.1 1.4 %copy.23 = f32[1,128,4]{2,1,0:T(8,128)} copy(f32[1,128,4]{1,2,0:T(4,128)} %param.32) | data formatting | bytes 4096 | tf_op args[11]
  3.5 129.4 %shard_map.199 = bf16[128,2048]{1,0:T(8,128)(2,1)} custom-call(bf16[128,16,128]{2,1,0:T(8,128)(2,1)} %bitcast.20, bf16[128,16,128]{2,1,0:T(8,128)(2,1)} %bitcast.21, bf16[128,16,128]{2,1,0:T(8,128)(2,1)} %bitcast.22, f32[1]{0:T(128)S(6)} %copy.25.lam_ref, f32[1,128]{1,0:T(1,128)} %bitcast.29, bf16[128,2048]{1,0:T(8,128)(2,1)} %bitcast.23, ...), custom_call_target="tpu_custom_call" | custom-call | tf_op jit(solution)/shard_map/pallas_call | solution.py:325
  132.9 1.9 %copy.26 = bf16[1,128,2048]{2,1,0:T(8,128)(2,1)} copy(bf16[1,128,2048]{2,1,0:T(8,128)(2,1)} %bitcast.16) | data formatting | bytes 1048576

commit v2 on v1

v2 whole, which is shorter than its diff:
```python
import functools

import jax
import jax.numpy as jnp
import numpy as np
from jax import lax
from jax.experimental import pallas as pl
from jax.experimental.pallas import tpu as pltpu
from jax.sharding import PartitionSpec as P

MESH = pl.DeviceIdType.MESH
EPS = 1e-06
F32, BF16, I32 = jnp.float32, jnp.bfloat16, jnp.int32


def digits(k):
    return k // 32, (k // 8) % 4, (k // 2) % 4, k % 2


def link_load(k):
    load = np.zeros(6)
    dz, dy, dx, _ = digits(k)
    for i, d in enumerate((dx, dy, dz)):
        if d in (1, 2):
            load[2 * i] += 1
        if d in (2, 3):
            load[2 * i + 1] += 1
    return load


def first_link(k):
    dz, dy, dx, _ = digits(k)
    for i, d in enumerate((dx, dy, dz)):
        if d:
            return i, d
    return 3, 0


def balanced_order(offsets):
    left, total, out, last = list(offsets), np.zeros(6), [], None
    while left:

        def cost(k):
            t = total + link_load(k)
            return t.max() - t.min() + (0.5 if last is not None and first_link(k) == last else 0)

        k = min(left, key=cost)
        left.remove(k)
        out.append(k)
        total = total + link_load(k)
        last = first_link(k)
    return out


SP_ORDER = [k // 8 for k in balanced_order([8 * s for s in range(1, 16)])]
ALL_ORDER = [0] + balanced_order(range(1, 128))


def shifted(sp, dp, k, sign):
    dz, dy, dx, dc = digits(k)
    if sign < 0:
        dz, dy, dx, dc = -dz % 4, -dy % 4, -dx % 4, -dc % 2
    rem = lax.rem
    nsp = rem(sp // 4 + dz, 4) * 4 + rem(rem(sp, 4) + dy, 4)
    ndp = rem(dp // 2 + dx, 4) * 2 + rem(rem(dp, 2) + dc, 2)
    return nsp, ndp


def landed(ref, sem):
    pltpu.make_async_copy(ref, ref, sem).wait()


def dot(a, b):
    return jnp.dot(a, b, preferred_element_type=F32)


def rms(v, gain):
    return v * lax.rsqrt(jnp.mean(v * v, axis=-1, keepdims=True) + EPS) * gain


def layer_kernel(
    q_ref, k_ref, v_ref, lam_ref, hgain_ref, res_ref, mixg_ref, preg_ref, postg_ref,
    routes_ref, rw_ref, order_ref, perm_ref, permt_ref, turn_ref,
    wo_hbm, eg_hbm, eu_hbm, ed_hbm, sg_hbm, su_hbm, sd_hbm,
    out_ref,
    wo, wg, wu, wd,
    qkv_send, qkv_recv, p1, l1, mixture, head_send, head_recv, acc,
    x4, pick, slab_send, slab_recv, res_recv, xs, upd, shared, r0b, rwb,
    wsem, qs_sem, qr_sem, hs_sem, hr_sem, ds_sem, dr_sem, rs_sem, rr_sem, entered,
):
    sp, dp = lax.axis_index("sp"), lax.axis_index("dp")
    barrier = pltpu.get_barrier_semaphore()
    for d in range(1, 16):
        to, _ = shifted(sp, dp, 8 * d, 1)
        pl.semaphore_signal(barrier, inc=1, device_id=(to, dp), device_id_type=MESH)
    for d in range(1, 8):
        _, to = shifted(sp, dp, d, 1)
        pl.semaphore_signal(barrier, inc=1, device_id=(sp, to), device_id_type=MESH)

    def weights(i, src, dst):
        return pltpu.make_async_copy(src, dst, wsem.at[i])

    loads = [weights(0, wo_hbm, wo), weights(1, sg_hbm, wg), weights(2, su_hbm, wu), weights(3, sd_hbm, wd)]
    expert_loads = [weights(4, eg_hbm, wg), weights(5, eu_hbm, wu), weights(6, ed_hbm, wd)]

    turn = turn_ref[...]
    for g in range(8):
        at = slice(16 * g, 16 * (g + 1))
        q, k, v = (ref[at].reshape(256, 128) for ref in (q_ref, k_ref, v_ref))
        both = jnp.concatenate([q[:, :64], k[:, :64], q[:, 64:], k[:, 64:], v], axis=1)
        rows = dot(turn, both).astype(BF16)
        for part in range(3):
            qkv_send[part, :, at, :] = rows[:, part * 128 : (part + 1) * 128].reshape(16, 16, 128)
    pl.semaphore_wait(barrier, 22)
    for part in range(3):
        for i, d in enumerate(SP_ORDER):
            to, _ = shifted(sp, dp, 8 * d, 1)
            pltpu.make_async_remote_copy(
                qkv_send.at[part, to], qkv_recv.at[part, sp], qs_sem.at[part, i], qr_sem.at[part, i],
                device_id=(to, dp), device_id_type=MESH,
            ).start()
    for d in range(1, 8):
        _, to = shifted(sp, dp, d, 1)
        pl.semaphore_signal(entered, inc=1, device_id=(sp, to), device_id_type=MESH)
    for load in loads:
        load.start()
    for part in range(3):
        qkv_recv[part, sp] = qkv_send[part, sp]

    oz, oy, ox, oc = (order_ref[i : i + 1, :] for i in range(4))
    mz, my, mx, mc = sp // 4, lax.rem(sp, 4), dp // 2, lax.rem(dp, 2)
    expert = ((oz + mz) & 3) * 32 + ((oy + my) & 3) * 8 + ((ox + mx) & 3) * 2 + ((oc + mc) & 1)
    row_i = lax.broadcasted_iota(I32, (128, 128), 0)
    col_i = lax.broadcasted_iota(I32, (128, 128), 1)
    eye = col_i == row_i

    def as_column(row):
        return jnp.sum(jnp.where(eye, row, jnp.zeros_like(row)), axis=1, keepdims=True)

    hots = [as_column(routes_ref[j : j + 1, :].astype(F32)).astype(I32) == expert for j in range(4)]
    members = sum(h.astype(F32) for h in hots).astype(BF16)
    earlier = dot((col_i < row_i).astype(F32).astype(BF16), members)
    place = earlier + 24.0 * col_i.astype(F32)
    rows_j = []
    for j in range(4):
        r0 = jnp.sum(jnp.where(hots[j], place, 0.0), axis=1, keepdims=True)
        r0b[j] = jnp.broadcast_to(r0, (128, 128)).astype(I32)
        rwb[j] = jnp.broadcast_to(as_column(rw_ref[j : j + 1, :]), (128, 128))
        r0_row = jnp.sum(jnp.where(eye, r0, 0.0), axis=0, keepdims=True).astype(I32)
        rows_j.append(jnp.concatenate([r0_row + 6 * q for q in range(4)], axis=1))

    @pl.loop(0, 24)
    def _(c):
        base = pl.multiple_of(c * 128, 128)
        row = lax.broadcasted_iota(I32, (128, 512), 0) + base
        hit = (row == rows_j[0]) | (row == rows_j[1]) | (row == rows_j[2]) | (row == rows_j[3])
        pick[pl.ds(base, 128), :] = jnp.where(hit, 1.0, 0.0).astype(BF16)

    coef = 0.125 * 1.4426950408889634
    causal = lax.broadcasted_iota(I32, (256, 256), 1) <= lax.broadcasted_iota(I32, (256, 256), 0)

    def exponents(part, t):
        qk = qkv_recv[part, 2 * t : 2 * t + 2].reshape(256, 128)
        q = jnp.concatenate([jnp.zeros((256, 64), BF16), qk[:, :64]], axis=1)
        keys = qkv_recv[part, 0 : 2 * t + 2].reshape(256 * (t + 1), 128)
        s = lax.dot_general(q, keys, (((1,), (1,)), ((), ())), preferred_element_type=F32)
        diag = jnp.where(causal, s[:, t * 256 :], -1e30)
        s = diag if t == 0 else jnp.concatenate([s[:, : t * 256], diag], axis=1)
        p = jnp.exp2((s - jnp.max(s, axis=1, keepdims=True)) * coef)
        return p, jnp.sum(p, axis=1, keepdims=True)

    def tri(t):
        return t * (t + 1) // 2

    for i in range(15):
        landed(qkv_recv.at[0, 0], qr_sem.at[0, i])
    for t in range(8):
        p, l = exponents(0, t)
        l1[t] = jnp.broadcast_to(1.0 / l, (256, 128))
        for c in range(t + 1):
            p1[tri(t) + c] = p[:, c * 256 : (c + 1) * 256]
    for i in range(15):
        landed(qkv_recv.at[1, 0], qr_sem.at[1, i])
    lam = lam_ref[0]
    for t in range(8):
        p, l = exponents(1, t)
        scale1 = jnp.concatenate([l1[t], l1[t]], axis=1)
        scale2 = lam / l
        for c in range(t + 1):
            mixture[tri(t) + c] = (p1[tri(t) + c] * scale1 - p[:, c * 256 : (c + 1) * 256] * scale2).astype(BF16)
    for i in range(15):
        landed(qkv_recv.at[2, 0], qr_sem.at[2, i])
    for t in range(8):
        m = jnp.concatenate([mixture[tri(t) + c] for c in range(t + 1)], axis=1)
        o = dot(m, qkv_recv[2, 0 : 2 * t + 2].reshape(256 * (t + 1), 128))
        head_send[2 * t : 2 * t + 2] = rms(o, hgain_ref[...]).astype(BF16).reshape(2, 128, 128)
    for i, d in enumerate(SP_ORDER):
        to, _ = shifted(sp, dp, 8 * d, 1)
        pltpu.make_async_remote_copy(
            head_send.at[to], head_recv.at[sp], hs_sem.at[i], hr_sem.at[i],
            device_id=(to, dp), device_id_type=MESH,
        ).start()
    head_recv[sp] = head_send[sp]

    loads[0].wait()
    sources = [sp] + [shifted(sp, dp, 8 * d, -1)[0] for d in SP_ORDER]
    for i in range(0, 16, 2):
        for n in (i, i + 1):
            if n:
                landed(head_recv.at[0], hr_sem.at[n - 1])
        h0, h1 = sources[i], sources[i + 1]
        x = jnp.concatenate([head_recv[h0], head_recv[h1]], axis=1)
        for c in range(4):
            cols = pl.ds(c * 512, 512)
            part = dot(x, jnp.concatenate([wo[h0, :, cols], wo[h1, :, cols]], axis=0))
            if i == 0:
                acc[:, cols] = part
            else:
                acc[:, cols] += part

    updated = (res_ref[...].astype(F32) + rms(acc[...], mixg_ref[...])).astype(BF16)
    upd[...] = updated
    normed = rms(updated.astype(F32), preg_ref[...]).astype(BF16)
    for q in range(4):
        x4[q * 128 : (q + 1) * 128, :] = normed[:, q * 512 : (q + 1) * 512]

    pl.semaphore_wait(entered, 7)
    for g in range(8):
        rows = dot(pick[g * 384 : (g + 1) * 384, :], x4[...]).astype(BF16)
        slab_send[g * 16 : (g + 1) * 16] = rows.reshape(16, 24, 512)
        for at in range(max(1, 16 * g), 16 * g + 16):
            pltpu.make_async_remote_copy(
                slab_send.at[at], slab_recv.at[at], ds_sem.at[0], dr_sem.at[at // 32],
                device_id=shifted(sp, dp, ALL_ORDER[at], 1), device_id_type=MESH,
            ).start()
    slab_recv[0] = slab_send[0]

    def hidden_of(x):
        gate, up = dot(x, wg[...]), dot(x, wu[...])
        return (gate / (1.0 + jnp.exp(-gate)) * up).astype(BF16)

    for load in loads[1:]:
        load.wait()
    shared_h = hidden_of(jnp.concatenate([x4[q * 128 : (q + 1) * 128, :] for q in range(4)], axis=1))
    shared[...] = dot(shared_h, wd[...]).astype(BF16)
    for load in expert_loads:
        load.start()

    @pl.loop(0, 12)
    def _(c):
        for half in range(2):
            col = lax.broadcasted_iota(I32, (128, 128), 1) + (c * 256 + half * 128)
            for q in range(4):
                w = jnp.zeros((128, 128), F32)
                for j in range(4):
                    w = jnp.where(col == r0b[j] + 6 * q, rwb[j], w)
                p1[(q // 2) * 12 + c, pl.ds((q % 2) * 128, 128), pl.ds(half * 128, 128)] = w

    for load in expert_loads:
        load.wait()

    @pl.loop(0, 4)
    def _(g):
        for gs in range(4):

            @pl.when(g == gs)
            def _():
                lo = max(1, 32 * gs)
                landed(slab_recv.at[pl.ds(lo, 32 * gs + 32 - lo)], dr_sem.at[gs])

        for b in range(4):
            block = slab_recv[pl.ds(g * 32 + b * 8, 8)].reshape(192, 512)
            y = dot(perm_ref[...], block).astype(BF16)
            for q in range(4):
                xs[b * 48 : (b + 1) * 48, q * 512 : (q + 1) * 512] = y[q * 48 : (q + 1) * 48]
        h = hidden_of(xs[...])
        xs[...] = dot(h, wd[...]).astype(BF16)
        for b in range(4):
            y = jnp.concatenate(
                [xs[b * 48 : (b + 1) * 48, q * 512 : (q + 1) * 512] for q in range(4)], axis=0
            )
            back = dot(permt_ref[...], y).astype(BF16)
            slab_recv[pl.ds(g * 32 + b * 8, 8)] = back.reshape(8, 24, 512)
        for gs in range(4):

            @pl.when(g == gs)
            def _():
                for at in range(max(1, 32 * gs), 32 * gs + 32):
                    pltpu.make_async_remote_copy(
                        slab_recv.at[at], res_recv.at[at], rs_sem.at[0], rr_sem.at[gs],
                        device_id=shifted(sp, dp, ALL_ORDER[at], -1), device_id_type=MESH,
                    ).start()

    res_recv[0] = slab_recv[0]

    for g in range(4):
        lo = max(1, 32 * g)
        landed(res_recv.at[pl.ds(lo, 32 * g + 32 - lo)], rr_sem.at[g])
        rows = res_recv[g * 32 : (g + 1) * 32].reshape(768, 512)
        for qq in range(2):
            w = jnp.concatenate([p1[qq * 12 + 3 * g + c] for c in range(3)], axis=1)
            hi = w.astype(BF16)
            part = dot(hi, rows) + dot((w - hi.astype(F32)).astype(BF16), rows)
            for q in range(2):
                at = pl.ds((2 * qq + q) * 512, 512)
                if g == 0:
                    acc[:, at] = part[q * 128 : (q + 1) * 128]
                else:
                    acc[:, at] += part[q * 128 : (q + 1) * 128]
    combined = acc[...] + shared[...].astype(F32)
    out_ref[...] = (upd[...].astype(F32) + rms(combined, postg_ref[...])).astype(BF16)

    for i in range(15):
        for part in range(3):
            landed(qkv_send.at[part, 0], qs_sem.at[part, i])
        landed(head_send.at[0], hs_sem.at[i])
    landed(slab_send.at[pl.ds(1, 127)], ds_sem.at[0])
    landed(slab_recv.at[pl.ds(1, 127)], rs_sem.at[0])


def local(
    queries, key_vectors, value_vectors, head_lambda, head_gain, residual, out_weight, mix_gain, pre_gain,
    post_gain, routes, route_weights, expert_gate, expert_up, expert_down, shared_gate, shared_up, shared_down,
):
    order = np.zeros((8, 128), np.int32)
    order[:4] = np.array([digits(k) for k in ALL_ORDER]).T
    perm = np.zeros((192, 192), np.float32)
    for src in range(8):
        for q in range(4):
            for s in range(6):
                perm[q * 48 + src * 6 + s, src * 24 + q * 6 + s] = 1
    turn = np.zeros((256, 256), np.float32)
    for h in range(16):
        for t in range(16):
            turn[h * 16 + t, t * 16 + h] = 1
    vm, hbm = pl.BlockSpec(memory_space=pltpu.VMEM), pl.BlockSpec(memory_space=pl.ANY)
    dma = pltpu.SemaphoreType.DMA
    slabs = pltpu.VMEM((128, 24, 512), BF16)
    out = pl.pallas_call(
        layer_kernel,
        out_shape=jax.ShapeDtypeStruct((128, 2048), BF16),
        in_specs=[vm, vm, vm, pl.BlockSpec(memory_space=pltpu.SMEM)] + [vm] * 11 + [hbm] * 7,
        out_specs=vm,
        scratch_shapes=[
            pltpu.VMEM((16, 128, 2048), BF16),
            pltpu.VMEM((2048, 512), BF16), pltpu.VMEM((2048, 512), BF16), pltpu.VMEM((512, 2048), BF16),
            pltpu.VMEM((3, 16, 128, 128), BF16), pltpu.VMEM((3, 16, 128, 128), BF16),
            pltpu.VMEM((36, 256, 256), F32), pltpu.VMEM((8, 256, 128), F32), pltpu.VMEM((36, 256, 256), BF16),
            pltpu.VMEM((16, 128, 128), BF16), pltpu.VMEM((16, 128, 128), BF16),
            pltpu.VMEM((128, 2048), F32),
            pltpu.VMEM((512, 512), BF16), pltpu.VMEM((3072, 512), BF16),
            slabs, slabs, slabs,
            pltpu.VMEM((192, 2048), BF16), pltpu.VMEM((128, 2048), BF16), pltpu.VMEM((128, 2048), BF16),
            pltpu.VMEM((4, 128, 128), I32), pltpu.VMEM((4, 128, 128), F32),
            dma((7,)), dma((3, 15)), dma((3, 15)), dma((15,)), dma((15,)), dma((1,)), dma((4,)), dma((1,)), dma((4,)),
            pltpu.SemaphoreType.REGULAR,
        ],
        compiler_params=pltpu.CompilerParams(
            collective_id=0, has_side_effects=True, vmem_limit_bytes=67043328
        ),
    )(
        queries[0], key_vectors[0], value_vectors[0], head_lambda, head_gain.reshape(1, 128), residual[0],
        mix_gain.reshape(1, -1), pre_gain.reshape(1, -1), post_gain.reshape(1, -1), routes[0].T, route_weights[0].T,
        jnp.asarray(order), jnp.asarray(perm, BF16), jnp.asarray(perm.T, BF16), jnp.asarray(turn, BF16),
        out_weight.reshape(16, 128, 2048), expert_gate[0], expert_up[0], expert_down[0],
        shared_gate, shared_up, shared_down,
    )
    return out.reshape(1, 128, 2048)


def solution(mesh):
    tokens, heads, experts = P("dp", "sp", None), P("dp", "sp", None, None), P(("sp", "dp"), None, None)
    return jax.shard_map(
        local,
        mesh=mesh,
        in_specs=(
            heads, heads, heads, P("sp"), P(), tokens, P(), P(), P(), P(), tokens, tokens,
            experts, experts, experts, P(), P(), P(),
        ),
        out_specs=tokens,
        check_vma=False,
    )
```

time: 135 us -> 119 us (0.88)
  Pallas kernels: 129 us -> 116 us
  local copies, waits for them, and re-layouts: 4.7 us -> 1.88 us
    pallas_call x1, Pallas kernels: 129 us -> 116 us  [local(): pl.pallas_call(layer_kernel, out_shape=jax.ShapeDtypeStruct((128, 2048),...]
    unnamed x3 -> x1, local copies, waits for them, and re-layouts: 4.7 us -> 1.88 us
where the time goes in v2:
time: 119 us; the launch traced here: 118 us
  Pallas kernels  116 us (97%)
  local copies, waits for them, and re-layouts  1.88 us (2%)
    pallas_call x1, Pallas kernels, local(): pl.pallas_call(layer_kernel, out_shape=jax.ShapeDtypeStruct((128, 2048),...  116 us

profile of v2, /device:TPU:1, one launch (start us, length us, event | category | flops | bytes accessed | tf_op | source)
XLA Modules:
  0.0 118.5 jit_solution(6687272207133353403)
XLA Ops:
  0.7 115.9 %shard_map.208 = bf16[128,2048]{1,0:T(8,128)(2,1)} custom-call(bf16[128,16,128]{2,1,0:T(8,128)(2,1)} %bitcast.24, bf16[128,16,128]{2,1,0:T(8,128)(2,1)} %bitcast.25, bf16[128,16,128]{2,1,0:T(8,128)(2,1)} %bitcast.26, f32[1]{0:T(128)S(6)} %copy.24.lam_ref, f32[1,128]{1,0:T(1,128)} %bitcast.33, bf16[128,2048]{1,0:T(8,128)(2,1)} %bitcast.27, ...), custom_call_target="tpu_custom_call" | custom-call | tf_op jit(solution)/shard_map/pallas_call | solution.py:339
  116.6 1.9 %copy.25 = bf16[1,128,2048]{2,1,0:T(8,128)(2,1)} copy(bf16[1,128,2048]{2,1,0:T(8,128)(2,1)} %bitcast.23) | data formatting | bytes 1048576

commit v3 on v2

--- a/solution.py
+++ b/solution.py
@@ -1,5 +1,3 @@
-import functools
-
 import jax
 import jax.numpy as jnp
 import numpy as np
@@ -56,14 +54,23 @@
 ALL_ORDER = [0] + balanced_order(range(1, 128))
 
 
-def shifted(sp, dp, k, sign):
-    dz, dy, dx, dc = digits(k)
-    if sign < 0:
-        dz, dy, dx, dc = -dz % 4, -dy % 4, -dx % 4, -dc % 2
-    rem = lax.rem
-    nsp = rem(sp // 4 + dz, 4) * 4 + rem(rem(sp, 4) + dy, 4)
-    ndp = rem(dp // 2 + dx, 4) * 2 + rem(rem(dp, 2) + dc, 2)
-    return nsp, ndp
+class Peers:
+    def __init__(self, sp, dp):
+        rem = lax.rem
+        z, y, x, c = sp // 4, rem(sp, 4), dp // 2, rem(dp, 2)
+        self.z = [4 * z] + [4 * rem(z + i, 4) for i in (1, 2, 3)]
+        self.y = [y] + [rem(y + i, 4) for i in (1, 2, 3)]
+        self.x = [2 * x] + [2 * rem(x + i, 4) for i in (1, 2, 3)]
+        self.c = [c, 1 - c]
+
+    def at(self, k, sign=1):
+        dz, dy, dx, dc = digits(k)
+        if sign < 0:
+            dz, dy, dx = -dz % 4, -dy % 4, -dx % 4
+        return self.z[dz] + self.y[dy], self.x[dx] + self.c[dc]
+
+    def sp(self, d, sign=1):
+        return self.at(8 * d, sign)[0]
 
 
 def landed(ref, sem):
@@ -79,23 +86,36 @@
 
 
 def layer_kernel(
-    q_ref, k_ref, v_ref, lam_ref, hgain_ref, res_ref, mixg_ref, preg_ref, postg_ref,
-    routes_ref, rw_ref, order_ref, perm_ref, permt_ref, turn_ref,
+    lam_ref,
+    q_hbm, k_hbm, v_hbm, hgain_hbm, res_hbm, mixg_hbm, preg_hbm, postg_hbm,
+    routes_hbm, rw_hbm, order_hbm, perm_hbm, permt_hbm, turn_hbm,
     wo_hbm, eg_hbm, eu_hbm, ed_hbm, sg_hbm, su_hbm, sd_hbm,
     out_ref,
+    q_ref, k_ref, v_ref, hgain_ref, res_ref, mixg_ref, preg_ref, postg_ref,
+    routes_ref, rw_ref, order_ref, perm_ref, permt_ref, turn_ref,
     wo, wg, wu, wd,
     qkv_send, qkv_recv, p1, l1, mixture, head_send, head_recv, acc,
-    x4, pick, slab_send, slab_recv, res_recv, xs, upd, shared, r0b, rwb,
-    wsem, qs_sem, qr_sem, hs_sem, hr_sem, ds_sem, dr_sem, rs_sem, rr_sem, entered,
+    x4, pick, slab_send, slab_recv, res_recv, xs, shared, r0b, rwb,
+    wsem, isem, qs_sem, qr_sem, hs_sem, hr_sem, ds_sem, dr_sem, rs_sem, rr_sem, entered,
 ):
     sp, dp = lax.axis_index("sp"), lax.axis_index("dp")
+    peers = Peers(sp, dp)
     barrier = pltpu.get_barrier_semaphore()
-    for d in range(1, 16):
-        to, _ = shifted(sp, dp, 8 * d, 1)
-        pl.semaphore_signal(barrier, inc=1, device_id=(to, dp), device_id_type=MESH)
-    for d in range(1, 8):
-        _, to = shifted(sp, dp, d, 1)
-        pl.semaphore_signal(barrier, inc=1, device_id=(sp, to), device_id_type=MESH)
+    for k in [8 * d for d in range(1, 16)] + list(range(1, 8)):
+        pl.semaphore_signal(barrier, inc=1, device_id=peers.at(k), device_id_type=MESH)
+    inputs = [
+        pltpu.make_async_copy(src, dst, isem.at[i])
+        for i, (src, dst) in enumerate(
+            (
+                (q_hbm, q_ref), (k_hbm, k_ref), (v_hbm, v_ref), (turn_hbm, turn_ref),
+                (routes_hbm, routes_ref), (rw_hbm, rw_ref), (order_hbm, order_ref),
+                (hgain_hbm, hgain_ref), (res_hbm, res_ref), (mixg_hbm, mixg_ref), (preg_hbm, preg_ref),
+                (postg_hbm, postg_ref), (perm_hbm, perm_ref), (permt_hbm, permt_ref),
+            )
+        )
+    ]
+    for load in inputs:
+        load.start()
 
     def weights(i, src, dst):
         return pltpu.make_async_copy(src, dst, wsem.at[i])
@@ -103,6 +123,8 @@
     loads = [weights(0, wo_hbm, wo), weights(1, sg_hbm, wg), weights(2, su_hbm, wu), weights(3, sd_hbm, wd)]
     expert_loads = [weights(4, eg_hbm, wg), weights(5, eu_hbm, wu), weights(6, ed_hbm, wd)]
 
+    for load in inputs[:4]:
+        load.wait()
     turn = turn_ref[...]
     for g in range(8):
         at = slice(16 * g, 16 * (g + 1))
@@ -114,19 +136,20 @@
     pl.semaphore_wait(barrier, 22)
     for part in range(3):
         for i, d in enumerate(SP_ORDER):
-            to, _ = shifted(sp, dp, 8 * d, 1)
+            to = peers.sp(d)
             pltpu.make_async_remote_copy(
                 qkv_send.at[part, to], qkv_recv.at[part, sp], qs_sem.at[part, i], qr_sem.at[part, i],
                 device_id=(to, dp), device_id_type=MESH,
             ).start()
     for d in range(1, 8):
-        _, to = shifted(sp, dp, d, 1)
-        pl.semaphore_signal(entered, inc=1, device_id=(sp, to), device_id_type=MESH)
+        pl.semaphore_signal(entered, inc=1, device_id=peers.at(d), device_id_type=MESH)
     for load in loads:
         load.start()
     for part in range(3):
         qkv_recv[part, sp] = qkv_send[part, sp]
 
+    for load in inputs[4:]:
+        load.wait()
     oz, oy, ox, oc = (order_ref[i : i + 1, :] for i in range(4))
     mz, my, mx, mc = sp // 4, lax.rem(sp, 4), dp // 2, lax.rem(dp, 2)
     expert = ((oz + mz) & 3) * 32 + ((oy + my) & 3) * 8 + ((ox + mx) & 3) * 2 + ((oc + mc) & 1)
@@ -195,19 +218,19 @@
         o = dot(m, qkv_recv[2, 0 : 2 * t + 2].reshape(256 * (t + 1), 128))
         head_send[2 * t : 2 * t + 2] = rms(o, hgain_ref[...]).astype(BF16).reshape(2, 128, 128)
     for i, d in enumerate(SP_ORDER):
-        to, _ = shifted(sp, dp, 8 * d, 1)
+        to = peers.sp(d)
         pltpu.make_async_remote_copy(
-            head_send.at[to], head_recv.at[sp], hs_sem.at[i], hr_sem.at[i],
+            head_send.at[to], head_recv.at[sp], hs_sem.at[i + 1], hr_sem.at[i + 1],
             device_id=(to, dp), device_id_type=MESH,
         ).start()
     head_recv[sp] = head_send[sp]
 
     loads[0].wait()
-    sources = [sp] + [shifted(sp, dp, 8 * d, -1)[0] for d in SP_ORDER]
+    sources = [sp] + [peers.sp(d, -1) for d in SP_ORDER]
     for i in range(0, 16, 2):
         for n in (i, i + 1):
             if n:
-                landed(head_recv.at[0], hr_sem.at[n - 1])
+                landed(head_recv.at[0], hr_sem.at[n])
         h0, h1 = sources[i], sources[i + 1]
         x = jnp.concatenate([head_recv[h0], head_recv[h1]], axis=1)
         for c in range(4):
@@ -219,7 +242,7 @@
                 acc[:, cols] += part
 
     updated = (res_ref[...].astype(F32) + rms(acc[...], mixg_ref[...])).astype(BF16)
-    upd[...] = updated
+    res_ref[...] = updated
     normed = rms(updated.astype(F32), preg_ref[...]).astype(BF16)
     for q in range(4):
         x4[q * 128 : (q + 1) * 128, :] = normed[:, q * 512 : (q + 1) * 512]
@@ -231,7 +254,7 @@
         for at in range(max(1, 16 * g), 16 * g + 16):
             pltpu.make_async_remote_copy(
                 slab_send.at[at], slab_recv.at[at], ds_sem.at[0], dr_sem.at[at // 32],
-                device_id=shifted(sp, dp, ALL_ORDER[at], 1), device_id_type=MESH,
+                device_id=peers.at(ALL_ORDER[at]), device_id_type=MESH,
             ).start()
     slab_recv[0] = slab_send[0]
 
@@ -258,6 +281,10 @@
 
     for load in expert_loads:
         load.wait()
+    for i in range(15):
+        for part in range(3):
+            landed(qkv_send.at[part, 0], qs_sem.at[part, i])
+        landed(head_send.at[0], hs_sem.at[i + 1])
 
     @pl.loop(0, 4)
     def _(g):
@@ -287,33 +314,32 @@
             def _():
                 for at in range(max(1, 32 * gs), 32 * gs + 32):
                     pltpu.make_async_remote_copy(
-                        slab_recv.at[at], res_recv.at[at], rs_sem.at[0], rr_sem.at[gs],
-                        device_id=shifted(sp, dp, ALL_ORDER[at], -1), device_id_type=MESH,
+                        slab_recv.at[at], res_recv.at[at], rs_sem.at[0], rr_sem.at[at // 16],
+                        device_id=peers.at(ALL_ORDER[at], -1), device_id_type=MESH,
                     ).start()
 
     res_recv[0] = slab_recv[0]
 
-    for g in range(4):
-        lo = max(1, 32 * g)
-        landed(res_recv.at[pl.ds(lo, 32 * g + 32 - lo)], rr_sem.at[g])
-        rows = res_recv[g * 32 : (g + 1) * 32].reshape(768, 512)
+    for u in range(8):
+        lo = max(1, 16 * u)
+        landed(res_recv.at[pl.ds(lo, 16 * u + 16 - lo)], rr_sem.at[u])
+        rows = res_recv[u * 16 : (u + 1) * 16].reshape(384, 512)
         for qq in range(2):
-            w = jnp.concatenate([p1[qq * 12 + 3 * g + c] for c in range(3)], axis=1)
+            blocks = [divmod(3 * u + c, 2) for c in range(3)]
+            w = jnp.concatenate(
+                [p1[qq * 12 + b, :, half * 128 : (half + 1) * 128] for b, half in blocks], axis=1
+            )
             hi = w.astype(BF16)
             part = dot(hi, rows) + dot((w - hi.astype(F32)).astype(BF16), rows)
             for q in range(2):
                 at = pl.ds((2 * qq + q) * 512, 512)
-                if g == 0:
+                if u == 0:
                     acc[:, at] = part[q * 128 : (q + 1) * 128]
                 else:
                     acc[:, at] += part[q * 128 : (q + 1) * 128]
     combined = acc[...] + shared[...].astype(F32)
-    out_ref[...] = (upd[...].astype(F32) + rms(combined, postg_ref[...])).astype(BF16)
-
-    for i in range(15):
-        for part in range(3):
-            landed(qkv_send.at[part, 0], qs_sem.at[part, i])
-        landed(head_send.at[0], hs_sem.at[i])
+    out_ref[...] = (res_ref[...].astype(F32) + rms(combined, postg_ref[...])).astype(BF16)
+
     landed(slab_send.at[pl.ds(1, 127)], ds_sem.at[0])
     landed(slab_recv.at[pl.ds(1, 127)], rs_sem.at[0])
 
@@ -336,12 +362,16 @@
     vm, hbm = pl.BlockSpec(memory_space=pltpu.VMEM), pl.BlockSpec(memory_space=pl.ANY)
     dma = pltpu.SemaphoreType.DMA
     slabs = pltpu.VMEM((128, 24, 512), BF16)
+    heads, wide = pltpu.VMEM((128, 16, 128), BF16), pltpu.VMEM((1, 2048), F32)
     out = pl.pallas_call(
         layer_kernel,
         out_shape=jax.ShapeDtypeStruct((128, 2048), BF16),
-        in_specs=[vm, vm, vm, pl.BlockSpec(memory_space=pltpu.SMEM)] + [vm] * 11 + [hbm] * 7,
+        in_specs=[pl.BlockSpec(memory_space=pltpu.SMEM)] + [hbm] * 21,
         out_specs=vm,
         scratch_shapes=[
+            heads, heads, heads, pltpu.VMEM((1, 128), F32), pltpu.VMEM((128, 2048), BF16),
+            wide, wide, wide, pltpu.VMEM((4, 128), I32), pltpu.VMEM((4, 128), F32), pltpu.VMEM((8, 128), I32),
+            pltpu.VMEM((192, 192), BF16), pltpu.VMEM((192, 192), BF16), pltpu.VMEM((256, 256), BF16),
             pltpu.VMEM((16, 128, 2048), BF16),
             pltpu.VMEM((2048, 512), BF16), pltpu.VMEM((2048, 512), BF16), pltpu.VMEM((512, 2048), BF16),
             pltpu.VMEM((3, 16, 128, 128), BF16), pltpu.VMEM((3, 16, 128, 128), BF16),
@@ -350,16 +380,16 @@
             pltpu.VMEM((128, 2048), F32),
             pltpu.VMEM((512, 512), BF16), pltpu.VMEM((3072, 512), BF16),
             slabs, slabs, slabs,
-            pltpu.VMEM((192, 2048), BF16), pltpu.VMEM((128, 2048), BF16), pltpu.VMEM((128, 2048), BF16),
+            pltpu.VMEM((192, 2048), BF16), pltpu.VMEM((128, 2048), BF16),
             pltpu.VMEM((4, 128, 128), I32), pltpu.VMEM((4, 128, 128), F32),
-            dma((7,)), dma((3, 15)), dma((3, 15)), dma((15,)), dma((15,)), dma((1,)), dma((4,)), dma((1,)), dma((4,)),
+            dma((7,)), dma((14,)), dma((3, 15)), dma((3, 15)), dma((16,)), dma((16,)), dma((1,)), dma((4,)), dma((1,)), dma((8,)),
             pltpu.SemaphoreType.REGULAR,
         ],
         compiler_params=pltpu.CompilerParams(
             collective_id=0, has_side_effects=True, vmem_limit_bytes=67043328
         ),
     )(
-        queries[0], key_vectors[0], value_vectors[0], head_lambda, head_gain.reshape(1, 128), residual[0],
+        head_lambda, queries[0], key_vectors[0], value_vectors[0], head_gain.reshape(1, 128), residual[0],
         mix_gain.reshape(1, -1), pre_gain.reshape(1, -1), post_gain.reshape(1, -1), routes[0].T, route_weights[0].T,
         jnp.asarray(order), jnp.asarray(perm, BF16), jnp.asarray(perm.T, BF16), jnp.asarray(turn, BF16),
         out_weight.reshape(16, 128, 2048), expert_gate[0], expert_up[0], expert_down[0],

time: 119 us -> 117 us (0.983)
    pallas_call x1, Pallas kernels: 116 us -> 115 us  [local(): pl.pallas_call(layer_kernel, out_shape=jax.ShapeDtypeStruct((128, 2048),...]
where the time goes in v3:
time: 117 us
  Pallas kernels  115 us (98%)
  local copies, waits for them, and re-layouts  1.88 us (2%)
    pallas_call x1, Pallas kernels, local(): pl.pallas_call(layer_kernel, out_shape=jax.ShapeDtypeStruct((128, 2048),...  115 us

profile of v3, /device:TPU:1, one launch (start us, length us, event | category | flops | bytes accessed | tf_op | source)
XLA Modules:
  0.0 117.2 jit_solution(13885071997624683580)
XLA Ops:
  0.7 114.6 %shard_map.208 = bf16[128,2048]{1,0:T(8,128)(2,1)} custom-call(f32[1]{0:T(128)S(6)} %copy.24.lam_ref, bf16[128,16,128]{2,1,0:T(8,128)(2,1)} %bitcast.24, bf16[128,16,128]{2,1,0:T(8,128)(2,1)} %bitcast.25, bf16[128,16,128]{2,1,0:T(8,128)(2,1)} %bitcast.26, f32[1,128]{1,0:T(1,128)} %bitcast.33, bf16[128,2048]{1,0:T(8,128)(2,1)} %bitcast.27, ...), custom_call_target="tpu_custom_call" | custom-call | tf_op jit(solution)/shard_map/pallas_call | solution.py:366
  115.3 1.9 %copy.25 = bf16[1,128,2048]{2,1,0:T(8,128)(2,1)} copy(bf16[1,128,2048]{2,1,0:T(8,128)(2,1)} %bitcast.23) | data formatting | bytes 1048576

commit v4 on v3

--- a/solution.py
+++ b/solution.py
@@ -51,7 +51,7 @@
 
 
 SP_ORDER = [k // 8 for k in balanced_order([8 * s for s in range(1, 16)])]
-ALL_ORDER = [0] + balanced_order(range(1, 128))
+ALL_ORDER = [0] + [int(v) for v in np.random.RandomState(4).permutation(np.arange(1, 128))]
 
 
 class Peers:

time: 117 us -> 116 us (level)
  Pallas kernels: 115 us -> 113 us
    pallas_call x1, Pallas kernels: 115 us -> 113 us  [local(): pl.pallas_call(layer_kernel, out_shape=jax.ShapeDtypeStruct((128, 2048),...]
where the time goes in v4:
time: 116 us
  Pallas kernels  113 us (97%)
  local copies, waits for them, and re-layouts  1.88 us (2%)
    pallas_call x1, Pallas kernels, local(): pl.pallas_call(layer_kernel, out_shape=jax.ShapeDtypeStruct((128, 2048),...  113 us

profile of v4, /device:TPU:1, one launch (start us, length us, event | category | flops | bytes accessed | tf_op | source)
XLA Modules:
  0.0 116.0 jit_solution(13293305774189499390)
XLA Ops:
  0.7 113.4 %shard_map.208 = bf16[128,2048]{1,0:T(8,128)(2,1)} custom-call(f32[1]{0:T(128)S(6)} %copy.24.lam_ref, bf16[128,16,128]{2,1,0:T(8,128)(2,1)} %bitcast.24, bf16[128,16,128]{2,1,0:T(8,128)(2,1)} %bitcast.25, bf16[128,16,128]{2,1,0:T(8,128)(2,1)} %bitcast.26, f32[1,128]{1,0:T(1,128)} %bitcast.33, bf16[128,2048]{1,0:T(8,128)(2,1)} %bitcast.27, ...), custom_call_target="tpu_custom_call" | custom-call | tf_op jit(solution)/shard_map/pallas_call | solution.py:366
  114.1 1.9 %copy.25 = bf16[1,128,2048]{2,1,0:T(8,128)(2,1)} copy(bf16[1,128,2048]{2,1,0:T(8,128)(2,1)} %bitcast.23) | data formatting | bytes 1048576
